TPU v7x, 32 devices: a whole 2x2x4 slice. The times are simulated.
32 devices in a mesh: gr: 2 (over x), fs: 4 (over z), tp: 4 (over y, core).
Axes of the slice: x: 2, y: 2, z: 4, core: 2. Of those that a mesh axis runs over, the one named last changes fastest.
Arguments:
- prompt_tokens: bfloat16 [4096, 2048], P(('gr', 'fs', 'tp')), may hold values from -60 to 60
- norm_gain: float32 [2048], P(('gr', 'fs')), may hold values from 0.1 to 1.9
- up_master: float32 [2048, 8192], P(('gr', 'fs'), 'tp'), may hold values from -0.125 to 0.125
- down_master: float32 [2048, 8192], P(('gr', 'fs'), 'tp'), may hold values from -0.0625 to 0.0625
Outputs:
- up_served: bfloat16 [2048, 8192], P(None, 'tp')
- down_served: bfloat16 [2048, 8192], P(None, 'tp')
- mlp_output: bfloat16 [4096, 2048], P(('gr', 'fs', 'tp'))
All inputs are finite; a program needn't handle non-finite values.
Results may differ from a plain program's by a relative error of at most 0.014.
Values may be sent and summed in bfloat16 or wider, within the bound.
A program may use at most 128 MiB of HBM per device.

v0:
```python
import jax
import jax.numpy as jnp
from jax import lax
from jax.sharding import PartitionSpec as P


def on_device(prompt_tokens, norm_gain, up_master, down_master):
    up_local = (up_master * norm_gain[:, None]).astype(jnp.bfloat16)
    down_local = down_master.astype(jnp.bfloat16)
    up_served, down_served = (
        lax.all_gather(up_local, ("gr", "fs"), axis=0, tiled=True),
        lax.all_gather(down_local, ("gr", "fs"), axis=0, tiled=True),
    )
    floats = prompt_tokens.astype(jnp.float32)
    mean_square = jnp.mean(floats * floats, axis=1, keepdims=True)
    normed = (floats * lax.rsqrt(mean_square + 1e-06)).astype(jnp.bfloat16)
    pre = jnp.dot(
        lax.all_gather(normed, "tp", axis=0, tiled=True),
        up_served,
        preferred_element_type=jnp.float32,
    )
    hidden = jnp.square(jnp.maximum(pre, 0.0)).astype(jnp.bfloat16)
    mlp_output = lax.psum_scatter(
        lax.dot_general(
            hidden, down_served, (((1,), (1,)), ((), ())), preferred_element_type=jnp.float32
        ).astype(jnp.bfloat16),
        "tp",
        scatter_dimension=0,
        tiled=True,
    )
    return (up_served, down_served, mlp_output)


def solution(mesh):
    placed = (
        P(("gr", "fs", "tp"), None),
        P(("gr", "fs")),
        P(("gr", "fs"), "tp"),
        P(("gr", "fs"), "tp"),
    )
    return jax.shard_map(
        on_device,
        mesh=mesh,
        in_specs=placed,
        out_specs=(P(None, "tp"), P(None, "tp"), P(("gr", "fs", "tp"), None)),
        check_vma=False,
    )
```

profile of v0, /device:TPU:0, one launch (start us, length us, event | category | flops | bytes accessed | tf_op | source)
XLA Modules:
  0.0 358.0 jit_solution(9934953560371709461)
XLA Ops:
  7.2 0.0 copy-start
  7.2 0.0 all-gather.8.cloned.1.call-start
  7.2 1.4 fusion
  8.6 2.0 fusion.1
  10.6 0.0 all-gather.8.cloned.1.call-update
  10.6 0.0 all-gather.4.cloned.1.call-start
  10.7 2.7 multiply_convert_fusion.1
  13.4 0.0 all-gather.4.cloned.1.call-update
  13.4 0.0 all-gather.6.cloned.1.call-start
  13.5 0.0 copy-done
  13.5 1.1 convert_element_type.19
  14.6 0.0 all-gather.6.cloned.1.call-update
  14.6 0.0 reduce-scatter.2.cloned.1.call-start
  14.7 21.4 %all-gather.8.cloned.1.call-done = bf16[512,2048]{1,0:T(8,128)(2,1)} async-done(((bf16[128,2048]{1,0:T(8,128)(2,1)}), bf16[512,2048]{1,0:T(8,128)(2,1)}) %all-gather.8.cloned.1.call-update) | async-done | bytes 2097168 | tf_op jit(solution)/shard_map/all_gather | solution.py:18
  36.1 127.2 %all-gather.4.cloned.1.call-done = bf16[2048,2048]{1,0:T(8,128)(2,1)} async-done(((bf16[256,2048]{1,0:T(8,128)(2,1)}), bf16[2048,2048]{1,0:T(8,128)(2,1)}) %all-gather.4.cloned.1.call-update) | async-done | bytes 8388624 | tf_op jit(solution)/shard_map/all_gather | solution.py:11
  163.2 125.4 %all-gather.6.cloned.1.call-done = bf16[2048,2048]{1,0:T(8,128)(2,1)} async-done(((bf16[256,2048]{1,0:T(8,128)(2,1)}), bf16[2048,2048]{1,0:T(8,128)(2,1)}) %all-gather.6.cloned.1.call-update) | async-done | bytes 8388624 | tf_op jit(solution)/shard_map/all_gather | solution.py:12
  288.6 16.5 %convolution_convert_fusion = bf16[512,2048]{1,0:T(8,128)(2,1)} fusion(bf16[2048,2048]{1,0:T(8,128)(2,1)} %all-gather.6.cloned.1.call-done, bf16[512,2048]{1,0:T(8,128)(2,1)} %all-gather.8.cloned.1.call-done, bf16[2048,2048]{1,0:T(8,128)(2,1)} %all-gather.4.cloned.1.call-done), kind=kOutput, calls=%fused_computation.1 | convolution fusion | flops 8594128896 | bytes 20971520 | tf_op jit(solution)/shard_map/dot_general | solution.py:24
  305.1 0.0 reduce-scatter.2.cloned.1.call-update
  305.1 29.5 %reduce-scatter.2.cloned.1.call-done = bf16[128,2048]{1,0:T(8,128)(2,1)} async-done(((bf16[512,2048]{1,0:T(8,128)(2,1)}), bf16[128,2048]{1,0:T(8,128)(2,1)}) %reduce-scatter.2.cloned.1.call-update) | async-done | bytes 524304 | tf_op jit(solution)/shard_map/reduce_scatter | solution.py:23
  334.6 8.4 %copy.9 = bf16[2048,2048]{1,0:T(8,128)(2,1)} copy(bf16[2048,2048]{1,0:T(8,128)(2,1)} %all-gather.4.cloned.1.call-done) | data formatting | bytes 16777216
  343.1 8.4 %copy.10 = bf16[2048,2048]{1,0:T(8,128)(2,1)} copy(bf16[2048,2048]{1,0:T(8,128)(2,1)} %all-gather.6.cloned.1.call-done) | data formatting | bytes 16777216
  (1 shorter events, 0.0 us)
Async XLA Ops:
  7.2 6.3 %copy-start = (f32[256,2048]{1,0:T(8,128)S(1)}, f32[256,2048]{1,0:T(8,128)}, u32[]{:S(2)}) copy-start(f32[256,2048]{1,0:T(8,128)} %param.7) | copy-start | bytes 6291460
  7.2 28.9 %all-gather.8.cloned.1.call-start = ((), (), s32[]{:S(2)}) async-start(), calls=%async_computation.3 | async-start | bytes 2621440 | tf_op jit(solution)/shard_map/all_gather | solution.py:18
  10.6 152.6 %all-gather.4.cloned.1.call-start = ((), (), s32[]{:S(2)}) async-start(), calls=%async_computation.1 | async-start | bytes 9437184 | tf_op jit(solution)/shard_map/all_gather | solution.py:11
  13.4 275.2 %all-gather.6.cloned.1.call-start = ((), (), s32[]{:S(2)}) async-start(), calls=%async_computation.2 | async-start | bytes 9437184 | tf_op jit(solution)/shard_map/all_gather | solution.py:12
  14.6 320.0 %reduce-scatter.2.cloned.1.call-start = ((), (), s32[]{:S(2)}) async-start(), calls=%async_computation.4 | async-start | bytes 2621440 | tf_op jit(solution)/shard_map/reduce_scatter | solution.py:23
Sparse Core Ops, SparseCore 0:
  10.7 25.2 all-gather.7
  38.8 124.4 all-gather.3
  165.9 122.6 all-gather.5
  305.3 29.3 reduce-scatter.1
where the time goes:
time: 358 us
  waiting for transfers between devices  303 us (85%)
  local copies, waits for them, and re-layouts  16.9 us (5%)
  matrix products  16.5 us (5%)
  between operations  13.8 us (4%)
  other arithmetic  7.23 us (2%)
    all_gather x1, waiting for transfers between devices, on_device(): lax.all_gather(up_local, ('gr', 'fs'), axis=0, tiled=True)  127 us
    all_gather x1, waiting for transfers between devices, on_device(): lax.all_gather(down_local, ('gr', 'fs'), axis=0, tiled=True)  125 us
    reduce_scatter x1, waiting for transfers between devices, on_device(): lax.psum_scatter(lax.dot_general(hidden, down_served, (((1,), (1,)), ((),...  29.5 us
    all_gather x1, waiting for transfers between devices, on_device(): lax.all_gather(normed, 'tp', axis=0, tiled=True)  21.4 us
    unnamed x4, local copies, waits for them, and re-layouts  16.9 us
    dot_general x1, matrix products, on_device(): lax.dot_general(hidden, down_served, (((1,), (1,)), ((), ())), preferred_...  16.5 us
  transfers between devices with their start and end apart: 4, of which 4 were waited for; matrix products, arithmetic and copies ran while one was open for 1% of the time, Pallas kernels for 0%

commit v1 on v0

v1 whole, which is shorter than its diff:
```python
import functools

import jax
import jax.numpy as jnp
from jax import lax
from jax.experimental import pallas as pl
from jax.experimental.pallas import tpu as pltpu
from jax.sharding import PartitionSpec as P

MESH = pl.DeviceIdType.MESH
CHUNK_BYTES = 128 * 1024


def pieces_of(rows, most):
    count = max(1, -(-rows // most))
    units = rows // 16
    cuts = [16 * (units * i // count) for i in range(count + 1)]
    return [(a, b - a) for a, b in zip(cuts, cuts[1:])]


def kernel(
    sizes, tok_hbm, gain_ref, up_hbm, down_hbm,
    up_ref, down_ref, out_ref,
    tok_ref, stage, normed, hidden, part, arrived,
    load_sem, tok_send, tok_recv,
    z_recv, right_send, left_send, x_recv, x_send, part_send, part_recv,
):
    n_gr, n_fs, n_tp = sizes
    g, z, t = lax.axis_index("gr"), lax.axis_index("fs"), lax.axis_index("tp")
    rows, width = stage.shape[1:]
    local = tok_ref.shape[0]
    depth = up_ref.shape[0]
    last = n_fs - 1
    has_right, has_left = z < last, z > 0
    masters = (up_ref, down_ref)

    def crossing(numerator):
        return max(16, rows * numerator // 256 * 16)

    most = max(16, CHUNK_BYTES // (2 * width) // 16 * 16)
    x_first = (crossing(3), crossing(2))
    tables = []
    for p in range(2):
        table = pieces_of(rows - x_first[p], most)
        tables.append(table + [(rows - x_first[p], x_first[p])] * 2)

    def at(p, col, zz, k):
        start, size = tables[p][k]
        base = pl.multiple_of((col * n_fs + zz) * rows, rows)
        return masters[p].at[pl.ds(pl.multiple_of(base + start, 16), size), :]

    def count(p):
        return len(tables[p]) - 2

    def z_copy(p, zz, k, right):
        col = 1 - g if k == count(p) + 1 else g
        ref = at(p, col, zz, k)
        send = right_send if right else left_send
        return pltpu.make_async_remote_copy(
            src_ref=ref, dst_ref=ref, send_sem=send.at[p, zz, k], recv_sem=z_recv.at[p, zz, k],
            device_id=(g, jnp.where(has_right, z + 1, z - 1) if right else jnp.where(has_left, z - 1, z + 1), t),
            device_id_type=MESH,
        )

    def x_copy(p, zz, k, col):
        ref = at(p, col, zz, k)
        return pltpu.make_async_remote_copy(
            src_ref=ref, dst_ref=ref, send_sem=x_send.at[p, zz, k], recv_sem=x_recv.at[p, zz, k],
            device_id=(1 - g, z, t), device_id_type=MESH,
        )

    def send_both(p, k):
        pl.when(has_right)(lambda: z_copy(p, z, k, True).start())
        pl.when(has_left)(lambda: z_copy(p, z, k, False).start())

    def own_z(p):
        for k in range(count(p) + 1):
            send_both(p, k)

    def own_x(p):
        x_copy(p, z, count(p), g).start()
        for k in range(count(p)):
            x_copy(p, z, k, g).start()

    def other_xz(p):
        x_copy(p, z, count(p), 1 - g).wait_recv()
        send_both(p, count(p) + 1)

    def slot(p, s):
        from_left, from_right = z - s >= 0, z + s <= last
        for k in range(count(p) + 2):
            def left_in():
                z_copy(p, z - s, k, True).wait_recv()
                if s < last:
                    pl.when(has_right)(lambda: z_copy(p, z - s, k, True).start())
                if k < count(p):
                    x_copy(p, z - s, k, g).start()

            def right_in():
                z_copy(p, z + s, k, False).wait_recv()
                if s < last:
                    pl.when(has_left)(lambda: z_copy(p, z + s, k, False).start())
                if k < count(p):
                    x_copy(p, z + s, k, g).start()

            pl.when(from_left)(left_in)
            pl.when(from_right)(right_in)

    def token_copy(j):
        mine = normed.at[pl.ds(pl.multiple_of(t * local, local), local), :]
        return pltpu.make_async_remote_copy(
            src_ref=mine, dst_ref=mine, send_sem=tok_send.at[j - 1], recv_sem=tok_recv.at[j - 1],
            device_id=(g, z, lax.rem(t + j, n_tp)), device_id_type=MESH,
        )

    def part_copy(block, j):
        to = lax.rem(t + j, n_tp)
        row = pl.ds(pl.multiple_of(block * rows, rows), rows)
        return pltpu.make_async_remote_copy(
            src_ref=part.at[row, pl.ds(pl.multiple_of(to * local, local), local)],
            dst_ref=arrived.at[j - 1, row, :],
            send_sem=part_send.at[block, j - 1], recv_sem=part_recv.at[block, j - 1],
            device_id=(g, z, to), device_id_type=MESH,
        )

    def second(s):
        def one(i, carry):
            other, side = i // 2, lax.rem(i, 2)
            dist = s - other
            zz = z + (2 * side - 1) * dist
            ok = (dist >= 0) & (zz >= 0) & (zz <= last) & ((dist > 0) | (side == 0))

            @pl.when(ok)
            def _():
                @pl.when(other == 1)
                def _():
                    for k in range(count(1)):
                        x_copy(1, zz, k, 1 - g).wait_recv()

                block = jnp.where(other == 1, 1 - g, g) * n_fs + zz
                row = pl.ds(pl.multiple_of(block * rows, rows), rows)
                part[row, :] = lax.dot_general(
                    down_ref[row, :], hidden[...], (((1,), (1,)), ((), ())),
                    preferred_element_type=jnp.float32,
                ).astype(part.dtype)
                for j in range(1, n_tp):
                    part_copy(block, j).start()

            return carry

        lax.fori_loop(0, 4, one, 0)

    loads = [
        pltpu.make_async_copy(up_hbm, stage.at[0], load_sem.at[0]),
        pltpu.make_async_copy(tok_hbm, tok_ref, load_sem.at[1]),
        pltpu.make_async_copy(down_hbm, stage.at[1], load_sem.at[2]),
    ]
    for load in loads:
        load.start()

    barrier = pltpu.get_barrier_semaphore()

    def greet(device):
        pl.semaphore_signal(barrier, inc=1, device_id=device, device_id_type=MESH)

    greet((1 - g, z, t))
    for j in range(1, n_tp):
        greet((g, z, lax.rem(t + j, n_tp)))
    pl.when(has_right)(lambda: greet((g, z + 1, t)))
    pl.when(has_left)(lambda: greet((g, z - 1, t)))

    own = pl.ds(pl.multiple_of((g * n_fs + z) * rows, rows), rows)
    loads[0].wait()
    up_ref[own, :] = (stage[0] * gain_ref[...]).astype(up_ref.dtype)
    pl.semaphore_wait(barrier, n_tp + has_right.astype(jnp.int32) + has_left.astype(jnp.int32))
    own_x(0)
    own_z(0)

    loads[1].wait()
    floats = tok_ref[...].astype(jnp.float32)
    mean_square = jnp.mean(floats * floats, axis=1, keepdims=True)
    normed[pl.ds(pl.multiple_of(t * local, local), local), :] = (
        floats * lax.rsqrt(mean_square + 1e-06)
    ).astype(normed.dtype)
    for j in range(1, n_tp):
        token_copy(j).start()
    other_xz(0)
    loads[2].wait()
    down_ref[own, :] = stage[1].astype(down_ref.dtype)

    for s in range(1, last):
        slot(0, s)
    own_z(1)
    if last > 0:
        slot(0, last)
    own_x(1)

    for zz in range(n_fs):
        for k in range(count(0)):
            x_copy(0, zz, k, 1 - g).wait_recv()
    for j in range(1, n_tp):
        token_copy(j).wait_recv()

    tile = 256

    def first(i, carry):
        columns = pl.ds(pl.multiple_of(i * tile, tile), tile)
        pre = jnp.dot(normed[...], up_ref[:, columns], preferred_element_type=jnp.float32)
        hidden[:, columns] = jnp.square(jnp.maximum(pre, 0.0)).astype(hidden.dtype)
        return carry

    lax.fori_loop(0, width // tile, first, 0)

    other_xz(1)
    second(0)
    for s in range(1, n_fs):
        slot(1, s)
        second(s)
    second(n_fs)

    def arrivals(b, carry):
        for j in range(1, n_tp):
            part_copy(b, j).wait_recv()
        return carry

    lax.fori_loop(0, n_gr * n_fs, arrivals, 0)

    def total(i, carry):
        row = pl.ds(pl.multiple_of(i * 128, 128), 128)
        acc = part[row, pl.ds(pl.multiple_of(t * local, local), local)].astype(jnp.float32)
        for j in range(1, n_tp):
            acc = acc + arrived[j - 1, row, :].astype(jnp.float32)
        out_ref[:, row] = acc.T.astype(out_ref.dtype)
        return carry

    lax.fori_loop(0, depth // 128, total, 0)

    def sent_parts(b, carry):
        for j in range(1, n_tp):
            part_copy(b, j).wait_send()
        return carry

    lax.fori_loop(0, n_gr * n_fs, sent_parts, 0)
    for j in range(1, n_tp):
        token_copy(j).wait_send()

    def sent_blocks(zz, carry):
        for p in range(2):
            for k in range(count(p) + 2):
                pl.when(has_right & (zz <= z))(lambda: z_copy(p, zz, k, True).wait_send())
                pl.when(has_left & (zz >= z))(lambda: z_copy(p, zz, k, False).wait_send())
                if k < count(p):
                    x_copy(p, zz, k, g).wait_send()
                elif k == count(p):
                    pl.when(zz == z)(lambda: x_copy(p, zz, k, g).wait_send())
        return carry

    lax.fori_loop(0, n_fs, sent_blocks, 0)


def solution(mesh):
    n_gr, n_fs, n_tp = (mesh.shape[a] for a in ("gr", "fs", "tp"))

    def on_device(prompt_tokens, norm_gain, up_master, down_master):
        local, depth = prompt_tokens.shape
        rows, width = up_master.shape
        blocks = n_gr * n_fs
        most = 2 + -(-rows // max(16, CHUNK_BYTES // (2 * width) // 16 * 16))
        dma = pltpu.SemaphoreType.DMA
        bf16 = jnp.bfloat16
        anywhere = pl.BlockSpec(memory_space=pl.ANY)
        vmem = pl.BlockSpec(memory_space=pltpu.VMEM)
        return pl.pallas_call(
            functools.partial(kernel, (n_gr, n_fs, n_tp)),
            out_shape=(
                pltpu.VMEM((depth, width), bf16),
                pltpu.VMEM((depth, width), bf16),
                jax.ShapeDtypeStruct((local, depth), bf16),
            ),
            in_specs=[anywhere, vmem, anywhere, anywhere],
            out_specs=(vmem, vmem, vmem),
            scratch_shapes=[
                pltpu.VMEM((local, depth), bf16),
                pltpu.VMEM((2, rows, width), jnp.float32),
                pltpu.VMEM((local * n_tp, depth), bf16),
                pltpu.VMEM((local * n_tp, width), bf16),
                pltpu.VMEM((depth, local * n_tp), bf16),
                pltpu.VMEM((n_tp - 1, depth, local), bf16),
                dma((3,)), dma((n_tp - 1,)), dma((n_tp - 1,)),
                dma((2, n_fs, most)), dma((2, n_fs, most)), dma((2, n_fs, most)),
                dma((2, n_fs, most)), dma((2, n_fs, most)),
                dma((blocks, n_tp - 1)), dma((blocks, n_tp - 1)),
            ],
            compiler_params=pltpu.CompilerParams(
                collective_id=0, has_side_effects=True, vmem_limit_bytes=44 * 2**20
            ),
        )(prompt_tokens, norm_gain[:, None], up_master, down_master)

    placed = (
        P(("gr", "fs", "tp"), None),
        P(("gr", "fs")),
        P(("gr", "fs"), "tp"),
        P(("gr", "fs"), "tp"),
    )
    return jax.shard_map(
        on_device,
        mesh=mesh,
        in_specs=placed,
        out_specs=(P(None, "tp"), P(None, "tp"), P(("gr", "fs", "tp"), None)),
        check_vma=False,
    )
```

time: 358 us -> 191 us (0.53)
  waiting for transfers between devices: 303 us -> 0 us
  Pallas kernels: 0 us -> 181 us
  matrix products: 16.5 us -> 0 us
  between operations: 13.8 us -> 0.64 us
  local copies, waits for them, and re-layouts: 16.9 us -> 9.07 us
  other arithmetic: 7.23 us -> 0 us
    all_gather x3 -> x0, waiting for transfers between devices: 274 us -> none  [the longest x1 127 us: on_device(): lax.all_gather(up_local, ('gr', 'fs'), axis=0, tiled=True)]
    pallas_call x0 -> x1, Pallas kernels: none -> 181 us  [on_device(): pl.pallas_call(functools.partial(kernel, (n_gr, n_fs, n_tp)), out_shape=(...]
    reduce_scatter x1 -> x0, waiting for transfers between devices: 29.5 us -> none  [on_device(): lax.psum_scatter(lax.dot_general(hidden, down_served, (((1,), (1,)), ((),...]
    dot_general x1 -> x0, matrix products: 16.5 us -> none  [on_device(): lax.dot_general(hidden, down_served, (((1,), (1,)), ((), ())), preferred_...]
    unnamed x4 -> x5, local copies, waits for them, and re-layouts: 16.9 us -> 7.59 us
    convert_element_type x3 -> x0, other arithmetic: 5.85 us -> none  [the longest x1 2.74 us: on_device(): up_local = (up_master * norm_gain[:, None]).astype(jnp.bfloat16)]
  transfers between devices with their start and end apart: 4 -> 0, of which waited for: 4 -> 0; matrix products, arithmetic and copies ran while one was open for 1% -> 0% of each run, Pallas kernels for 0% -> 0%
where the time goes in v1:
time: 191 us
  Pallas kernels  181 us (95%)
  local copies, waits for them, and re-layouts  9.07 us (5%)
    pallas_call x1, Pallas kernels, on_device(): pl.pallas_call(functools.partial(kernel, (n_gr, n_fs, n_tp)), out_shape=(...  181 us
    unnamed x5, local copies, waits for them, and re-layouts  7.59 us

profile of v1, /device:TPU:0, one launch (start us, length us, event | category | flops | bytes accessed | tf_op | source)
XLA Modules:
  0.0 190.7 jit_solution(1509412789592806650)
XLA Ops:
  0.6 1.5 copy.7.gain_ref
  2.1 181.0 %shard_map.67 = (bf16[2048,2048]{1,0:T(8,128)(2,1)S(1)}, bf16[2048,2048]{1,0:T(8,128)(2,1)S(1)}, bf16[128,2048]{1,0:T(8,128)(2,1)}) custom-call(bf16[128,2048]{1,0:T(8,128)(2,1)} %tok_hbm.1, f32[256,1]{1,0:T(8,128)} %copy.7.gain_ref, f32[256,2048]{1,0:T(8,128)} %up_hbm.1, f32[256,2048]{1,0:T(8,128)} %down_hbm.1), custom_call_target="tpu_custom_call" | custom-call | tf_op jit(solution)/shard_map/pallas_call | solution.py:273
  183.1 3.4 %copy.11 = bf16[2048,2048]{1,0:T(8,128)(2,1)} copy(bf16[2048,2048]{1,0:T(8,128)(2,1)S(1)} %get-tuple-element.3) | data formatting | bytes 16777216
  186.5 0.0 copy-start
  186.5 3.4 %copy.12 = bf16[2048,2048]{1,0:T(8,128)(2,1)} copy(bf16[2048,2048]{1,0:T(8,128)(2,1)S(1)} %get-tuple-element.4) | data formatting | bytes 16777216
  189.9 0.0 copy-done
  189.9 0.8 copy.13
Async XLA Ops:
  186.5 3.4 %copy-start = (bf16[128,2048]{1,0:T(8,128)(2,1)S(1)}, bf16[128,2048]{1,0:T(8,128)(2,1)}, u32[]{:S(2)}) copy-start(bf16[128,2048]{1,0:T(8,128)(2,1)} %get-tuple-element.11) | copy-start | bytes 1572868

commit v2 on v1

--- a/solution.py
+++ b/solution.py
@@ -86,9 +86,9 @@
         x_copy(p, z, count(p), 1 - g).wait_recv()
         send_both(p, count(p) + 1)
 
-    def slot(p, s):
+    def slot(p, s, items=None):
         from_left, from_right = z - s >= 0, z + s <= last
-        for k in range(count(p) + 2):
+        for k in range(count(p) + 2) if items is None else items:
             def left_in():
                 z_copy(p, z - s, k, True).wait_recv()
                 if s < last:
@@ -113,22 +113,41 @@
             device_id=(g, z, lax.rem(t + j, n_tp)), device_id_type=MESH,
         )
 
-    def part_copy(block, j):
+    far = jnp.where(z + z >= last, 0, last)
+    splits = (0, count(1) * 4 // 7, count(1) * 6 // 7, count(1))
+    starts = [tables[1][k][0] for k in splits[:3]] + [rows]
+    shares = [(a, b - a) for a, b in zip(starts, starts[1:])]
+    whole_block = (0, rows)
+
+    def part_copy(block, share, i, j):
         to = lax.rem(t + j, n_tp)
-        row = pl.ds(pl.multiple_of(block * rows, rows), rows)
+        start, size = share
+        base = pl.multiple_of(block * rows, rows)
+        row = pl.ds(pl.multiple_of(base + start, 16), size)
         return pltpu.make_async_remote_copy(
             src_ref=part.at[row, pl.ds(pl.multiple_of(to * local, local), local)],
             dst_ref=arrived.at[j - 1, row, :],
-            send_sem=part_send.at[block, j - 1], recv_sem=part_recv.at[block, j - 1],
+            send_sem=part_send.at[block, i, j - 1], recv_sem=part_recv.at[block, i, j - 1],
             device_id=(g, z, to), device_id_type=MESH,
         )
+
+    def multiply(block, share, i):
+        start, size = share
+        base = pl.multiple_of(block * rows, rows)
+        row = pl.ds(pl.multiple_of(base + start, 16), size)
+        part[row, :] = lax.dot_general(
+            down_ref[row, :], hidden[...], (((1,), (1,)), ((), ())),
+            preferred_element_type=jnp.float32,
+        ).astype(part.dtype)
+        for j in range(1, n_tp):
+            part_copy(block, share, i, j).start()
 
     def second(s):
         def one(i, carry):
             other, side = i // 2, lax.rem(i, 2)
             dist = s - other
             zz = z + (2 * side - 1) * dist
-            ok = (dist >= 0) & (zz >= 0) & (zz <= last) & ((dist > 0) | (side == 0))
+            ok = (dist >= 0) & (zz >= 0) & (zz <= last) & ((dist > 0) | (side == 0)) & (zz != far)
 
             @pl.when(ok)
             def _():
@@ -137,18 +156,48 @@
                     for k in range(count(1)):
                         x_copy(1, zz, k, 1 - g).wait_recv()
 
-                block = jnp.where(other == 1, 1 - g, g) * n_fs + zz
-                row = pl.ds(pl.multiple_of(block * rows, rows), rows)
-                part[row, :] = lax.dot_general(
-                    down_ref[row, :], hidden[...], (((1,), (1,)), ((), ())),
-                    preferred_element_type=jnp.float32,
-                ).astype(part.dtype)
-                for j in range(1, n_tp):
-                    part_copy(block, j).start()
+                multiply(jnp.where(other == 1, 1 - g, g) * n_fs + zz, whole_block, 0)
 
             return carry
 
         lax.fori_loop(0, 4, one, 0)
+
+    def far_share(col, i):
+        if shares[i][1] > 0:
+            multiply(col * n_fs + far, shares[i], i)
+
+    def far_x(i):
+        for k in range(splits[i], splits[i + 1]):
+            x_copy(1, far, k, 1 - g).wait_recv()
+
+    def far_blocks():
+        slot(1, last, range(splits[0], splits[1]))
+        second(last)
+        far_share(g, 0)
+        slot(1, last, range(splits[1], splits[2]))
+        far_x(0)
+        far_share(1 - g, 0)
+        far_share(g, 1)
+        slot(1, last, range(splits[2], splits[3] + 1))
+        far_share(g, 2)
+        far_x(1)
+        far_share(1 - g, 1)
+        slot(1, last, range(splits[3] + 1, splits[3] + 2))
+        far_x(2)
+        far_share(1 - g, 2)
+
+    def parts(b, act):
+        @pl.when(lax.rem(b, n_fs) == far)
+        def _():
+            for i in range(3):
+                if shares[i][1] > 0:
+                    for j in range(1, n_tp):
+                        act(part_copy(b, shares[i], i, j))
+
+        @pl.when(lax.rem(b, n_fs) != far)
+        def _():
+            for j in range(1, n_tp):
+                act(part_copy(b, whole_block, 0, j))
 
     loads = [
         pltpu.make_async_copy(up_hbm, stage.at[0], load_sem.at[0]),
@@ -170,8 +219,11 @@
     pl.when(has_left)(lambda: greet((g, z - 1, t)))
 
     own = pl.ds(pl.multiple_of((g * n_fs + z) * rows, rows), rows)
+    square = (rows, rows)
+    on_diagonal = lax.broadcasted_iota(jnp.int32, square, 0) == lax.broadcasted_iota(jnp.int32, square, 1)
+    gain = jnp.sum(jnp.where(on_diagonal, gain_ref[...], 0.0), axis=1, keepdims=True)
     loads[0].wait()
-    up_ref[own, :] = (stage[0] * gain_ref[...]).astype(up_ref.dtype)
+    up_ref[own, :] = (stage[0] * gain).astype(up_ref.dtype)
     pl.semaphore_wait(barrier, n_tp + has_right.astype(jnp.int32) + has_left.astype(jnp.int32))
     own_x(0)
     own_z(0)
@@ -213,17 +265,26 @@
 
     other_xz(1)
     second(0)
-    for s in range(1, n_fs):
+    for s in range(1, last):
         slot(1, s)
         second(s)
-    second(n_fs)
+    far_blocks()
+
+    final = (1 - g) * n_fs + far
+    last_tile = (final * rows + rows - 1) // 128
 
     def arrivals(b, carry):
-        for j in range(1, n_tp):
-            part_copy(b, j).wait_recv()
+        @pl.when(b != final)
+        def _():
+            parts(b, lambda copy: copy.wait_recv())
+
         return carry
 
     lax.fori_loop(0, n_gr * n_fs, arrivals, 0)
+    for i in range(2):
+        if shares[i][1] > 0:
+            for j in range(1, n_tp):
+                part_copy(final, shares[i], i, j).wait_recv()
 
     def total(i, carry):
         row = pl.ds(pl.multiple_of(i * 128, 128), 128)
@@ -233,11 +294,11 @@
         out_ref[:, row] = acc.T.astype(out_ref.dtype)
         return carry
 
-    lax.fori_loop(0, depth // 128, total, 0)
+    lax.fori_loop(0, last_tile, total, 0)
+    lax.fori_loop(last_tile + 1, depth // 128, total, 0)
 
     def sent_parts(b, carry):
-        for j in range(1, n_tp):
-            part_copy(b, j).wait_send()
+        parts(b, lambda copy: copy.wait_send())
         return carry
 
     lax.fori_loop(0, n_gr * n_fs, sent_parts, 0)
@@ -256,6 +317,10 @@
         return carry
 
     lax.fori_loop(0, n_fs, sent_blocks, 0)
+
+    for j in range(1, n_tp):
+        part_copy(final, shares[2], 2, j).wait_recv()
+    total(last_tile, 0)
 
 
 def solution(mesh):
@@ -289,12 +354,12 @@
                 dma((3,)), dma((n_tp - 1,)), dma((n_tp - 1,)),
                 dma((2, n_fs, most)), dma((2, n_fs, most)), dma((2, n_fs, most)),
                 dma((2, n_fs, most)), dma((2, n_fs, most)),
-                dma((blocks, n_tp - 1)), dma((blocks, n_tp - 1)),
+                dma((blocks, 3, n_tp - 1)), dma((blocks, 3, n_tp - 1)),
             ],
             compiler_params=pltpu.CompilerParams(
                 collective_id=0, has_side_effects=True, vmem_limit_bytes=44 * 2**20
             ),
-        )(prompt_tokens, norm_gain[:, None], up_master, down_master)
+        )(prompt_tokens, norm_gain[None, :], up_master, down_master)
 
     placed = (
         P(("gr", "fs", "tp"), None),

time: 191 us -> 188 us (0.984)
  no operation moved by 1% of the time
where the time goes in v2:
time: 188 us
  Pallas kernels  180 us (96%)
  local copies, waits for them, and re-layouts  7.59 us (4%)
    pallas_call x1, Pallas kernels, on_device(): pl.pallas_call(functools.partial(kernel, (n_gr, n_fs, n_tp)), out_shape=(...  180 us
    unnamed x5, local copies, waits for them, and re-layouts  7.59 us

profile of v2, /device:TPU:0, one launch (start us, length us, event | category | flops | bytes accessed | tf_op | source)
XLA Modules:
  0.0 188.0 jit_solution(8247455300887342054)
XLA Ops:
  0.6 179.8 %shard_map.67 = (bf16[2048,2048]{1,0:T(8,128)(2,1)S(1)}, bf16[2048,2048]{1,0:T(8,128)(2,1)S(1)}, bf16[128,2048]{1,0:T(8,128)(2,1)}) custom-call(bf16[128,2048]{1,0:T(8,128)(2,1)} %tok_hbm.1, f32[1,256]{1,0:T(1,128)} %bitcast.1, f32[256,2048]{1,0:T(8,128)} %up_hbm.1, f32[256,2048]{1,0:T(8,128)} %down_hbm.1), custom_call_target="tpu_custom_call" | custom-call | tf_op jit(solution)/shard_map/pallas_call | solution.py:338
  180.4 3.4 %copy.10 = bf16[2048,2048]{1,0:T(8,128)(2,1)} copy(bf16[2048,2048]{1,0:T(8,128)(2,1)S(1)} %get-tuple-element.3) | data formatting | bytes 16777216
  183.8 0.0 copy-start
  183.8 3.4 %copy.11 = bf16[2048,2048]{1,0:T(8,128)(2,1)} copy(bf16[2048,2048]{1,0:T(8,128)(2,1)S(1)} %get-tuple-element.4) | data formatting | bytes 16777216
  187.2 0.0 copy-done
  187.2 0.8 copy.12
Async XLA Ops:
  183.8 3.4 %copy-start = (bf16[128,2048]{1,0:T(8,128)(2,1)S(1)}, bf16[128,2048]{1,0:T(8,128)(2,1)}, u32[]{:S(2)}) copy-start(bf16[128,2048]{1,0:T(8,128)(2,1)} %get-tuple-element.11) | copy-start | bytes 1572868

commit v3 on v2

--- a/solution.py
+++ b/solution.py
@@ -8,7 +8,7 @@
 from jax.sharding import PartitionSpec as P
 
 MESH = pl.DeviceIdType.MESH
-CHUNK_BYTES = 128 * 1024
+CHUNK_BYTES = 256 * 1024
 
 
 def pieces_of(rows, most):
@@ -38,7 +38,7 @@
         return max(16, rows * numerator // 256 * 16)
 
     most = max(16, CHUNK_BYTES // (2 * width) // 16 * 16)
-    x_first = (crossing(3), crossing(2))
+    x_first = (crossing(3), crossing(3))
     tables = []
     for p in range(2):
         table = pieces_of(rows - x_first[p], most)
@@ -204,8 +204,8 @@
         pltpu.make_async_copy(tok_hbm, tok_ref, load_sem.at[1]),
         pltpu.make_async_copy(down_hbm, stage.at[1], load_sem.at[2]),
     ]
-    for load in loads:
-        load.start()
+    loads[0].start()
+    loads[1].start()
 
     barrier = pltpu.get_barrier_semaphore()
 
@@ -217,16 +217,32 @@
         greet((g, z, lax.rem(t + j, n_tp)))
     pl.when(has_right)(lambda: greet((g, z + 1, t)))
     pl.when(has_left)(lambda: greet((g, z - 1, t)))
+
+    def round_up(k):
+        start, size = tables[0][k]
+        row = pl.ds(pl.multiple_of((g * n_fs + z) * rows + start, 16), size)
+        up_ref[row, :] = (stage[0, start : start + size] * gain[start : start + size]).astype(up_ref.dtype)
+
+    def send_own(k):
+        x_copy(0, z, k, g).start()
+        if k < count(0):
+            send_both(0, k)
 
     own = pl.ds(pl.multiple_of((g * n_fs + z) * rows, rows), rows)
     square = (rows, rows)
     on_diagonal = lax.broadcasted_iota(jnp.int32, square, 0) == lax.broadcasted_iota(jnp.int32, square, 1)
     gain = jnp.sum(jnp.where(on_diagonal, gain_ref[...], 0.0), axis=1, keepdims=True)
     loads[0].wait()
-    up_ref[own, :] = (stage[0] * gain).astype(up_ref.dtype)
+    order = [count(0)] + list(range(count(0)))
+    round_up(order[0])
+    round_up(order[1])
     pl.semaphore_wait(barrier, n_tp + has_right.astype(jnp.int32) + has_left.astype(jnp.int32))
-    own_x(0)
-    own_z(0)
+    for i, k in enumerate(order):
+        send_own(k)
+        if i + 2 < len(order):
+            round_up(order[i + 2])
+    send_both(0, count(0))
+    loads[2].start()
 
     loads[1].wait()
     floats = tok_ref[...].astype(jnp.float32)

time: 188 us -> 183 us (0.973)
  Pallas kernels: 180 us -> 175 us
    pallas_call x1, Pallas kernels: 180 us -> 175 us  [on_device(): pl.pallas_call(functools.partial(kernel, (n_gr, n_fs, n_tp)), out_shape=(...]
where the time goes in v3:
time: 183 us
  Pallas kernels  175 us (96%)
  local copies, waits for them, and re-layouts  7.59 us (4%)
    pallas_call x1, Pallas kernels, on_device(): pl.pallas_call(functools.partial(kernel, (n_gr, n_fs, n_tp)), out_shape=(...  175 us
    unnamed x5, local copies, waits for them, and re-layouts  7.59 us

profile of v3, /device:TPU:0, one launch (start us, length us, event | category | flops | bytes accessed | tf_op | source)
XLA Modules:
  0.0 183.0 jit_solution(15150659070226047703)
XLA Ops:
  0.6 174.8 %shard_map.67 = (bf16[2048,2048]{1,0:T(8,128)(2,1)S(1)}, bf16[2048,2048]{1,0:T(8,128)(2,1)S(1)}, bf16[128,2048]{1,0:T(8,128)(2,1)}) custom-call(bf16[128,2048]{1,0:T(8,128)(2,1)} %tok_hbm.1, f32[1,256]{1,0:T(1,128)} %bitcast.1, f32[256,2048]{1,0:T(8,128)} %up_hbm.1, f32[256,2048]{1,0:T(8,128)} %down_hbm.1), custom_call_target="tpu_custom_call" | custom-call | tf_op jit(solution)/shard_map/pallas_call | solution.py:354
  175.4 3.4 %copy.10 = bf16[2048,2048]{1,0:T(8,128)(2,1)} copy(bf16[2048,2048]{1,0:T(8,128)(2,1)S(1)} %get-tuple-element.3) | data formatting | bytes 16777216
  178.8 0.0 copy-start
  178.8 3.4 %copy.11 = bf16[2048,2048]{1,0:T(8,128)(2,1)} copy(bf16[2048,2048]{1,0:T(8,128)(2,1)S(1)} %get-tuple-element.4) | data formatting | bytes 16777216
  182.2 0.0 copy-done
  182.2 0.8 copy.12
Async XLA Ops:
  178.8 3.4 %copy-start = (bf16[128,2048]{1,0:T(8,128)(2,1)S(1)}, bf16[128,2048]{1,0:T(8,128)(2,1)}, u32[]{:S(2)}) copy-start(bf16[128,2048]{1,0:T(8,128)(2,1)} %get-tuple-element.11) | copy-start | bytes 1572868
